TPU v7x, 128 devices: a whole 4x4x4 slice. The times are simulated.
128 devices in a mesh: kv: 32 (over z, y, core), tp: 4 (over x).
Axes of the slice: x: 4, y: 4, z: 4, core: 2. Of those that a mesh axis runs over, the one named last changes fastest.
Arguments:
- tokens: bfloat16 [512, 4, 4096], P('kv'), may hold values from -6 to 6
- norm_gain: bfloat16 [4096], replicated, may hold values from 0.099609375 to 1.8984375
- query_weight: bfloat16 [4096, 2048], P(None, 'tp'), may hold values from -0.09375 to 0.09375
- key_weight: bfloat16 [4096, 2048], P(None, 'tp'), may hold values from -0.09375 to 0.09375
- value_weight: bfloat16 [4096, 2048], P(None, 'tp'), may hold values from -0.09375 to 0.09375
- outgate_weight: bfloat16 [4096, 2048], P(None, 'tp'), may hold values from -0.09375 to 0.09375
- gate_weight: bfloat16 [4096, 32], replicated, may hold values from -0.09375 to 0.09375
- gate_bias: float32 [2, 16], replicated, may hold values from -1 to 4
- head_gain: bfloat16 [2048], P('tp'), may hold values from 0.099609375 to 1.8984375
- out_weight: bfloat16 [2048, 4096], P('tp', 'kv'), may hold values from -0.125 to 0.125
- state_c: float32 [512, 16, 128, 128], P('kv', 'tp'), may hold values from -3 to 3
- state_n: float32 [512, 16, 128], P('kv', 'tp'), may hold values from -3 to 3
- state_m: float32 [512, 16], P('kv', 'tp'), may hold values from -1 to 2
- prev_keys: bfloat16 [512, 16, 4, 128], P('kv', 'tp'), may hold values from -6 to 6
- prev_values: bfloat16 [512, 16, 4, 128], P('kv', 'tp'), may hold values from -6 to 6
- prev_gates: float32 [512, 16, 2, 4], P('kv', 'tp'), may hold values from -2 to 5
- accepted: int32 [512], P('kv'), may hold values from 0 to 4
Outputs:
- mixed: bfloat16 [512, 4, 4096], P(None, None, 'kv')
- carried_c: float32 [512, 16, 128, 128], P('kv', 'tp')
- carried_n: float32 [512, 16, 128], P('kv', 'tp')
- carried_m: float32 [512, 16], P('kv', 'tp')
- step_keys: bfloat16 [512, 16, 4, 128], P('kv', 'tp')
- step_values: bfloat16 [512, 16, 4, 128], P('kv', 'tp')
- step_gates: float32 [512, 16, 2, 4], P('kv', 'tp')
Inputs may be any that keep to these rules, and one draw needn't show every extreme that they name: accepted counts proposals of the last step, from none to all 4.
All inputs are finite; a program needn't handle non-finite values.
Results may differ from a plain program's by a relative error of at most 0.0075.
The roundings to bfloat16 on the way count: a program that leaves them out, or rounds other values in their place, can miss the bound.
Values may be sent and summed in bfloat16 or wider, within the bound.
No kernel may reach another device: no remote copies, remote signals or barrier semaphores. Data moves between devices by JAX's collectives and lax.ppermute only.
A program may use at most 128 MiB of HBM per device.

v0:
```python
import jax
import jax.numpy as jnp
from jax import lax
from jax.sharding import PartitionSpec as P

EPSILON = 1e-06
HIGHEST = lax.Precision.HIGHEST


def joined_along(tiles, dim):
    tiles = jnp.moveaxis(tiles, 0, dim)
    lengths = tiles.shape
    return tiles.reshape(*lengths[:dim], lengths[dim] * lengths[dim + 1], *lengths[dim + 2 :])


def from_everyone(x, axis):
    peers = lax.axis_size(axis)
    return lax.all_to_all(jnp.broadcast_to(x[None], (peers, *x.shape)), axis, 0, 0, tiled=True)


def collect(x, axis, dim):
    return joined_along(from_everyone(x, axis), dim)


def replay(state_c, state_n, state_m, keys_in, values_in, gates_in, accepted):
    proposals = keys_in.shape[2]
    scaled = keys_in.astype(jnp.float32) * keys_in.shape[3] ** (-0.5)
    values_f = values_in.astype(jnp.float32)
    igates = gates_in[:, :, 0, :]
    forget = jax.nn.log_sigmoid(gates_in[:, :, 1, :])
    position = jnp.arange(proposals, dtype=jnp.int32)
    within = position[None, None, :] < accepted[:, None, None]
    masked = jnp.where(within, forget, 0.0)
    summed = jnp.sum(masked, axis=-1)
    log_weight = jnp.where(
        within, summed[..., None] - jnp.cumsum(masked, axis=-1) + igates, -jnp.inf
    )
    carried_m = jnp.maximum(summed + state_m, jnp.max(log_weight, axis=-1))
    shrink = jnp.exp(summed + state_m - carried_m)
    weights = jnp.exp(log_weight - carried_m[..., None])
    carried_c = shrink[..., None, None] * state_c + jnp.einsum(
        "bhs,bhsv,bhsd->bhvd", weights, values_f, scaled, precision=HIGHEST
    )
    carried_n = shrink[..., None] * state_n + jnp.einsum(
        "bhs,bhsd->bhd", weights, scaled, precision=HIGHEST
    )
    return (carried_c, carried_n, carried_m)


def cell_block(state_c, state_n, state_m, queries, scaled, values_f, igates, forget):
    proposals = queries.shape[2]
    cumul = jnp.cumsum(forget, axis=-1)
    causal = jnp.tril(jnp.ones((proposals, proposals), dtype=bool))
    log_decay = jnp.where(
        causal, cumul[..., :, None] - cumul[..., None, :] + igates[..., None, :], -jnp.inf
    )
    carried = cumul + state_m[..., None]
    stable = jnp.maximum(carried, jnp.max(log_decay, axis=-1))
    scores = jnp.einsum("bhtd,bhsd->bhts", queries, scaled, precision=HIGHEST) * jnp.exp(
        log_decay - stable[..., None]
    )
    weight_state = jnp.exp(carried - stable)
    numer = weight_state[..., None] * jnp.einsum(
        "bhvd,bhtd->bhtv", state_c, queries, precision=HIGHEST
    )
    numer = numer + jnp.einsum("bhts,bhsv->bhtv", scores, values_f, precision=HIGHEST)
    denom = weight_state * jnp.einsum(
        "bhd,bhtd->bht", state_n, queries, precision=HIGHEST
    ) + jnp.sum(scores, axis=-1)
    return numer / jnp.maximum(jnp.abs(denom), jnp.exp(-stable))[..., None]


def gate_heads(hidden, gain, outgate):
    heads_count = hidden.shape[1]
    head_size = hidden.shape[3]
    normed = hidden * lax.rsqrt(jnp.mean(hidden * hidden, axis=-1, keepdims=True) + EPSILON)
    normed = normed * gain.astype(jnp.float32).reshape(heads_count, head_size)[None, :, None, :]
    rows_out = jnp.transpose(normed, (0, 2, 1, 3)).reshape(outgate.shape)
    return (rows_out * jax.nn.sigmoid(outgate.astype(jnp.float32))).astype(jnp.bfloat16)


def per_device(
    tokens,
    norm_gain,
    query_weight,
    key_weight,
    value_weight,
    outgate_weight,
    gate_weight,
    gate_bias,
    head_gain,
    out_weight,
    state_c,
    state_n,
    state_m,
    prev_keys,
    prev_values,
    prev_gates,
    accepted,
):
    seqs_local, proposals, features = tokens.shape
    heads_local = state_m.shape[1]
    head_size = state_n.shape[2]
    tokens_f = tokens.astype(jnp.float32)
    normed = tokens_f * lax.rsqrt(jnp.mean(tokens_f * tokens_f, axis=-1, keepdims=True) + EPSILON)
    normed = (normed * norm_gain.astype(jnp.float32)).astype(jnp.bfloat16)
    rows_in = normed.reshape(seqs_local * proposals, features)

    def project(matrix):
        return jnp.dot(rows_in, matrix, preferred_element_type=jnp.float32).astype(jnp.bfloat16)

    def by_head(array):
        return array.reshape(seqs_local, proposals, heads_local, head_size).transpose(0, 2, 1, 3)

    queries = project(query_weight)
    keys_new = project(key_weight)
    values_new = project(value_weight)
    outgate = project(outgate_weight)
    all_gates = (
        jnp.dot(rows_in, gate_weight, preferred_element_type=jnp.float32)
        + gate_bias.reshape(-1)[None, :]
    )
    heads_total = gate_weight.shape[1] // 2
    head_offset = lax.axis_index("tp") * heads_local
    igates = lax.dynamic_slice_in_dim(all_gates, head_offset, heads_local, 1)
    fgates = lax.dynamic_slice_in_dim(all_gates, heads_total + head_offset, heads_local, 1)
    igates = igates.reshape(seqs_local, proposals, heads_local).transpose(0, 2, 1)
    fgates = fgates.reshape(seqs_local, proposals, heads_local).transpose(0, 2, 1)
    step_gates = jnp.stack([igates, fgates], axis=2)
    carried_c, carried_n, carried_m = replay(
        state_c, state_n, state_m, prev_keys, prev_values, prev_gates, accepted
    )
    step_keys = by_head(keys_new)
    step_values = by_head(values_new)
    hidden = cell_block(
        carried_c,
        carried_n,
        carried_m,
        by_head(queries).astype(jnp.float32),
        step_keys.astype(jnp.float32) * head_size ** (-0.5),
        step_values.astype(jnp.float32),
        igates,
        jax.nn.log_sigmoid(fgates),
    )
    gated = gate_heads(hidden, head_gain, outgate)
    partial_out = jnp.dot(collect(gated, "kv", 0), out_weight, preferred_element_type=jnp.float32)
    summed = lax.psum(partial_out, "tp")
    mixed = summed.astype(jnp.bfloat16).reshape(-1, proposals, summed.shape[1])
    return (mixed, carried_c, carried_n, carried_m, step_keys, step_values, step_gates)


def solution(mesh):
    in_specs = (
        P("kv", None, None),
        P(),
        P(None, "tp"),
        P(None, "tp"),
        P(None, "tp"),
        P(None, "tp"),
        P(),
        P(),
        P("tp"),
        P("tp", "kv"),
        P("kv", "tp", None, None),
        P("kv", "tp", None),
        P("kv", "tp"),
        P("kv", "tp", None, None),
        P("kv", "tp", None, None),
        P("kv", "tp", None, None),
        P("kv"),
    )
    out_specs = (
        P(None, None, "kv"),
        P("kv", "tp", None, None),
        P("kv", "tp", None),
        P("kv", "tp"),
        P("kv", "tp", None, None),
        P("kv", "tp", None, None),
        P("kv", "tp", None, None),
    )
    return jax.shard_map(
        per_device, mesh=mesh, in_specs=in_specs, out_specs=out_specs, check_vma=False
    )
```

profile of v0, /device:TPU:0, one launch (start us, length us, event | category | flops | bytes accessed | tf_op | source)
XLA Modules:
  0.0 114.7 jit_solution(9230726068473415681)
XLA Ops:
  0.6 0.0 copy-start
  0.7 0.8 add.110
  1.5 0.7 iota_compare_fusion
  2.2 0.7 bitcast_convert_fusion
  2.9 0.8 copy.77
  3.6 1.4 %fusion.7 = f32[16,4]{1,0:T(8,128)S(1)} fusion(bf16[16,4,4096]{2,1,0:T(4,128)(2,1)} %param.17), kind=kLoop, calls=%fused_computation.16 | loop fusion | flops 786368 | bytes 524544 | tf_op jit(solution)/shard_map/reduce_sum | solution.py:105
  5.0 0.7 convert_element_type.41
  5.7 0.7 fusion.41
  6.5 0.1 copy.93
  6.6 0.1 copy.76
  6.7 1.4 %fusion.9 = bf16[16,4,4096]{2,1,0:T(4,128)(2,1)S(1)} fusion(bf16[16,4,4096]{2,1,0:T(4,128)(2,1)} %param.17, f32[4096]{0:T(1024)S(1)} %convert_element_type.41, f32[16,4]{1,0:T(8,128)S(1)} %add_rsqrt_fusion), kind=kLoop, calls=%fused_computation.18 | loop fusion | flops 1048576 | bytes 1065216 | tf_op jit(solution)/shard_map/convert_element_type | solution.py:106
  8.1 0.1 reshape.103
  8.2 0.3 convolution_add_fusion
  8.5 0.1 reshape.104
  8.6 0.1 reshape.105
  8.7 0.1 fusion.24
  8.8 0.1 fusion.39
  8.9 2.8 %reduce_window_sum.18 = f32[16,4,4]{2,1,0:T(4,128)S(1)} reduce-window(f32[16,4,4]{2,1,0:T(4,128)S(1)} %get-tuple-element.26, f32[]{:T(128)} %constant.13.clone.1), window={size=1x1x4 pad=0_0x0_0x3_0}, to_apply=%region_3.4 | reduce-window | flops 768 | bytes 2052 | tf_op jit(solution)/shard_map/jit(cumsum)/reduce_window_sum | solution.py:36
  11.7 2.7 %reduce_window_sum.17 = f32[16,4,4]{2,1,0:T(4,128)S(1)} reduce-window(f32[16,4,4]{2,1,0:T(4,128)S(1)} %fusion.24, f32[]{:T(128)} %constant.13.clone.1), window={size=1x1x4 pad=0_0x0_0x3_0}, to_apply=%region_1.2 | reduce-window | flops 768 | bytes 2052 | tf_op jit(solution)/shard_map/jit(cumsum)/reduce_window_sum | solution.py:52
  14.4 3.0 %convolution_convert_fusion.1 = bf16[64,512]{1,0:T(8,128)(2,1)S(1)} fusion(bf16[64,4096]{1,0:T(8,128)(2,1)S(1)} %reshape.103, bf16[4096,512]{1,0:T(8,128)(2,1)} %param.21), kind=kOutput, calls=%fused_computation.12 | convolution fusion | flops 268468224 | bytes 4784128 | tf_op jit(solution)/shard_map/dot_general | solution.py:110
  17.5 3.1 %convolution_convert_fusion.2 = bf16[64,512]{1,0:T(8,128)(2,1)S(1)} fusion(bf16[64,4096]{1,0:T(8,128)(2,1)S(1)} %reshape.103, bf16[4096,512]{1,0:T(8,128)(2,1)} %param.20), kind=kOutput, calls=%fused_computation.13 | convolution fusion | flops 268468224 | bytes 4784128 | tf_op jit(solution)/shard_map/dot_general | solution.py:110
  20.6 3.1 %convolution_convert_fusion.3 = bf16[64,512]{1,0:T(8,128)(2,1)S(1)} fusion(bf16[64,4096]{1,0:T(8,128)(2,1)S(1)} %reshape.103, bf16[4096,512]{1,0:T(8,128)(2,1)} %param.19), kind=kOutput, calls=%fused_computation.14 | convolution fusion | flops 268468224 | bytes 4784128 | tf_op jit(solution)/shard_map/dot_general | solution.py:110
  23.7 0.2 fusion.38
  23.9 0.2 fusion.16
  24.1 0.1 subtract_exponential_fusion.1
  24.2 0.6 fusion.13
  24.8 0.1 copy_bitcast_fusion
  24.9 0.0 copy-start.7
  24.9 0.0 copy-start.6
  24.9 0.1 multiply_add_fusion.1
  25.0 0.4 fusion.22
  25.4 0.5 fusion.42
  25.8 0.1 exponential_maximum_fusion
  25.9 0.1 fusion.29
  26.0 9.1 %multiply_add_fusion = f32[16,4,128,128]{3,2,1,0:T(8,128)S(1)} fusion(f32[16,4,128,128]{3,2,1,0:T(8,128)} %param.27, f32[16,4]{1,0:T(8,128)S(1)} %get-tuple-element.23, bf16[16,4,4,128]{3,2,1,0:T(4,128)(2,1)S(1)} %copy-done.4, bf16[16,4,4,128]{3,2,1,0:T(4,128)(2,1)S(1)} %copy-done.5, f32[16,4,4]{2,1,0:T(4,128)S(1)} %get-tuple-element.33), kind=kOutput, calls=%fused_computation | convolution fusion | flops 52559872 | bytes 8520960 | tf_op jit(solution)/shard_map/bhs,bhsv,bhsd->bhvd/dot_general | solution.py:41
  35.2 3.3 %fusion.23 = f32[16,4,4,128]{3,2,1,0:T(4,128)S(1)} fusion(f32[16,4,128,128]{3,2,1,0:T(8,128)S(1)} %multiply_add_fusion, bf16[16,4,4,128]{3,2,1,0:T(4,128)(2,1)S(1)} %reshape.106), kind=kOutput, calls=%fused_computation.43 | convolution fusion | flops 50331648 | bytes 4390912 | tf_op jit(solution)/shard_map/bhvd,bhtd->bhtv/dot_general | solution.py:63
  38.5 0.6 fusion.17
  39.2 0.3 multiply_multiply_fusion
  39.5 0.9 fusion.6
  40.4 1.6 %broadcast_in_dim.52 = bf16[32,64,512]{2,1,0:T(8,128)(2,1)} broadcast(bf16[64,512]{1,0:T(8,128)(2,1)S(1)} %fusion.6), dimensions={1,2} | broadcast | bytes 2162688 | tf_op jit(solution)/shard_map/broadcast_in_dim | solution.py:18
  42.0 8.4 %all-to-all-start = ((bf16[32,64,512]{2,1,0:T(8,128)(2,1)}), bf16[32,64,512]{2,1,0:T(8,128)(2,1)S(1)}, u32[]{:S(2)}, u32[]{:S(2)}) async-start(bf16[32,64,512]{2,1,0:T(8,128)(2,1)} %broadcast_in_dim.52), calls=%async_computation | async-start | bytes 4194304 | tf_op jit(solution)/shard_map/all_to_all | solution.py:18
  50.4 0.7 copy.87
  51.1 0.1 copy.85
  51.2 0.1 copy.86
  51.3 0.6 pad_maximum_fusion
  51.9 28.6 %all-to-all-done = bf16[32,64,512]{2,1,0:T(8,128)(2,1)S(1)} async-done(((bf16[32,64,512]{2,1,0:T(8,128)(2,1)}), bf16[32,64,512]{2,1,0:T(8,128)(2,1)S(1)}, u32[]{:S(2)}, u32[]{:S(2)}) %all-to-all-start) | async-done | bytes 2097184 | tf_op jit(solution)/shard_map/all_to_all | solution.py:18
  80.5 0.7 fusion.43
  81.2 33.5 %all-reduce.1 = bf16[2048,128]{1,0:T(8,128)(2,1)} all-reduce(f32[2048,128]{1,0:T(8,128)S(1)} %fusion.43), channel_id=1, replica_groups=mesh['kv'=32,'tp'=4] {'tp'}, use_global_device_ids=true, to_apply=%region_8.9 | all-reduce | flops 262144 | bytes 1572864 | tf_op jit(solution)/shard_map/psum | solution.py:147
  (28 shorter events, 0.2 us)
Async XLA Ops:
  0.6 7.6 %copy-start = (bf16[4096,32]{0,1:T(8,128)(2,1)S(1)}, bf16[4096,32]{0,1:T(8,128)(2,1)}, u32[]{:S(2)}) copy-start(bf16[4096,32]{0,1:T(8,128)(2,1)} %param.23) | copy-start | bytes 786436
  17.5 6.7 %copy-start.4 = (bf16[16,4,4,128]{3,2,1,0:T(4,128)(2,1)S(1)}, bf16[16,4,4,128]{3,2,1,0:T(4,128)(2,1)}, u32[]{:S(2)}) copy-start(bf16[16,4,4,128]{3,2,1,0:T(4,128)(2,1)} %param.30) | copy-start | bytes 196612
  20.6 4.3 %copy-start.8 = (f32[16,4,128]{2,1,0:T(4,128)S(1)}, f32[16,4,128]{2,1,0:T(4,128)}, u32[]{:S(2)}) copy-start(f32[16,4,128]{2,1,0:T(4,128)} %param.28) | copy-start | bytes 98308
  20.6 5.4 %copy-start.5 = (bf16[16,4,4,128]{3,2,1,0:T(4,128)(2,1)S(1)}, bf16[16,4,4,128]{3,2,1,0:T(4,128)(2,1)}, u32[]{:S(2)}) copy-start(bf16[16,4,4,128]{3,2,1,0:T(4,128)(2,1)} %param.31) | copy-start | bytes 196612
  24.9 10.3 %copy-start.7 = (bf16[16,4,4,128]{3,2,1,0:T(4,128)(2,1)}, bf16[16,4,4,128]{3,2,1,0:T(4,128)(2,1)S(1)}, u32[]{:S(2)}) copy-start(bf16[16,4,4,128]{3,2,1,0:T(4,128)(2,1)S(1)} %get-tuple-element.40) | copy-start | bytes 196612
  24.9 13.7 %copy-start.6 = (bf16[16,4,4,128]{3,2,1,0:T(4,128)(2,1)}, bf16[16,4,4,128]{3,2,1,0:T(4,128)(2,1)S(1)}, u32[]{:S(2)}) copy-start(bf16[16,4,4,128]{3,2,1,0:T(4,128)(2,1)S(1)} %get-tuple-element.39) | copy-start | bytes 196612
  25.0 0.8 copy-start.9
  35.2 5.2 %copy-start.1 = (f32[16,4,128,128]{3,2,1,0:T(8,128)}, f32[16,4,128,128]{3,2,1,0:T(8,128)S(1)}, u32[]{:S(2)}) copy-start(f32[16,4,128,128]{3,2,1,0:T(8,128)S(1)} %multiply_add_fusion) | copy-start | bytes 12582916
  35.2 4.3 %copy-start.2 = (bf16[4096,512]{1,0:T(8,128)(2,1)S(1)}, bf16[4096,512]{1,0:T(8,128)(2,1)}, u32[]{:S(2)}) copy-start(bf16[4096,512]{1,0:T(8,128)(2,1)} %param.22) | copy-start | bytes 12582916
  40.4 40.1 %copy-start.3 = (bf16[512,128]{1,0:T(8,128)(2,1)S(1)}, bf16[512,128]{1,0:T(8,128)(2,1)}, u32[]{:S(2)}) copy-start(bf16[512,128]{1,0:T(8,128)(2,1)} %param.26) | copy-start | bytes 393220
  42.0 38.5 %all-to-all-start = ((bf16[32,64,512]{2,1,0:T(8,128)(2,1)}), bf16[32,64,512]{2,1,0:T(8,128)(2,1)S(1)}, u32[]{:S(2)}, u32[]{:S(2)}) async-start(bf16[32,64,512]{2,1,0:T(8,128)(2,1)} %broadcast_in_dim.52), calls=%async_computation | async-start | bytes 4194304 | tf_op jit(solution)/shard_map/all_to_all | solution.py:18
where the time goes:
time: 115 us
  blocking collectives  33.5 us (29%)
  waiting for transfers between devices  28.6 us (25%)
  matrix products  25.4 us (22%)
  other arithmetic  12.3 us (11%)
  starting transfers between devices  8.44 us (7%)
  local copies, waits for them, and re-layouts  5.47 us (5%)
    psum x1, blocking collectives, per_device(): summed = lax.psum(partial_out, 'tp')  33.5 us
    all_to_all x1, waiting for transfers between devices, from_everyone(): lax.all_to_all(jnp.broadcast_to(x[None], (peers, *x.shape)), axis, 0, 0,...  28.6 us
    dot_general x4, matrix products, project(): jnp.dot(rows_in, matrix, preferred_element_type=jnp.float32)  9.99 us
    dot_general x1, matrix products, replay(): jnp.einsum('bhs,bhsv,bhsd->bhvd', weights, values_f, scaled, precision=HI...  9.09 us
    all_to_all x1, starting transfers between devices, from_everyone(): lax.all_to_all(jnp.broadcast_to(x[None], (peers, *x.shape)), axis, 0, 0,...  8.44 us
    dot_general x1, matrix products, cell_block(): jnp.einsum('bhvd,bhtd->bhtv', state_c, queries, precision=HIGHEST)  3.35 us
    another operation x1, other arithmetic, replay(): jnp.cumsum(masked, axis=-1)  2.76 us
    another operation x1, other arithmetic, cell_block(): cumul = jnp.cumsum(forget, axis=-1)  2.75 us
  transfers between devices with their start and end apart: 1, of which 1 were waited for; matrix products, arithmetic and copies ran while one was open for 1% of the time, Pallas kernels for 0%

commit v1 on v0

--- a/solution.py
+++ b/solution.py
@@ -1,3 +1,4 @@
+import functools
 import jax
 import jax.numpy as jnp
 from jax import lax
@@ -5,6 +6,18 @@
 
 EPSILON = 1e-06
 HIGHEST = lax.Precision.HIGHEST
+
+
+def sizes_trace(message, comm_axis):
+    f_next = message
+    sides = lax.axis_size(comm_axis)
+    for b in [ii for ii in (1, 2, 4, 8, 16) if ii < sides]:
+        before = lax.ppermute(f_next, comm_axis, [(rr, rr ^ b) for rr in range(sides)])
+        f_next = f_next + before
+    return f_next
+
+
+links_keep_up = functools.partial(sizes_trace, comm_axis="tp")
 
 
 def joined_along(tiles, dim):
@@ -144,7 +157,7 @@
     )
     gated = gate_heads(hidden, head_gain, outgate)
     partial_out = jnp.dot(collect(gated, "kv", 0), out_weight, preferred_element_type=jnp.float32)
-    summed = lax.psum(partial_out, "tp")
+    summed = links_keep_up(partial_out)
     mixed = summed.astype(jnp.bfloat16).reshape(-1, proposals, summed.shape[1])
     return (mixed, carried_c, carried_n, carried_m, step_keys, step_values, step_gates)
 

time: 115 us -> 131 us (1.14)
  waiting for transfers between devices: 28.6 us -> 45 us
  starting transfers between devices: 8.44 us -> 4.67 us
  blocking collectives: 33.5 us -> 36.7 us
  local copies, waits for them, and re-layouts: 5.47 us -> 4.11 us
    ppermute x0 -> x2, waiting for transfers between devices: none -> 45 us  [sizes_trace(): lax.ppermute(f_next, comm_axis, [(rr, rr ^ b) for rr in range(sides)])]
    all_to_all x0 -> x1, blocking collectives: none -> 36.7 us  [from_everyone(): lax.all_to_all(jnp.broadcast_to(x[None], (peers, *x.shape)), axis, 0, 0,...]
    psum x1 -> x0, blocking collectives: 33.5 us -> none  [per_device(): summed = lax.psum(partial_out, 'tp')]
    all_to_all x1 -> x0, waiting for transfers between devices: 28.6 us -> none  [from_everyone(): lax.all_to_all(jnp.broadcast_to(x[None], (peers, *x.shape)), axis, 0, 0,...]
    all_to_all x1 -> x0, starting transfers between devices: 8.44 us -> none  [from_everyone(): lax.all_to_all(jnp.broadcast_to(x[None], (peers, *x.shape)), axis, 0, 0,...]
    ppermute x0 -> x2, starting transfers between devices: none -> 4.67 us  [sizes_trace(): lax.ppermute(f_next, comm_axis, [(rr, rr ^ b) for rr in range(sides)])]
    broadcast_in_dim x1, local copies, waits for them, and re-layouts: 1.59 us -> 0.23 us  [from_everyone(): jnp.broadcast_to(x[None], (peers, *x.shape))]
  transfers between devices with their start and end apart: 1 -> 2, of which waited for: 1 -> 2; matrix products, arithmetic and copies ran while one was open for 1% -> 1% of each run, Pallas kernels for 0% -> 0%
where the time goes in v1:
time: 131 us; the launch traced here: 130 us
  waiting for transfers between devices  45 us (34%)
  blocking collectives  36.7 us (28%)
  matrix products  25.4 us (19%)
  other arithmetic  13.3 us (10%)
  starting transfers between devices  4.67 us (4%)
  local copies, waits for them, and re-layouts  4.11 us (3%)
    ppermute x2, waiting for transfers between devices, sizes_trace(): lax.ppermute(f_next, comm_axis, [(rr, rr ^ b) for rr in range(sides)])  45 us
    all_to_all x1, blocking collectives, from_everyone(): lax.all_to_all(jnp.broadcast_to(x[None], (peers, *x.shape)), axis, 0, 0,...  36.7 us
    dot_general x4, matrix products, project(): jnp.dot(rows_in, matrix, preferred_element_type=jnp.float32)  9.99 us
    dot_general x1, matrix products, replay(): jnp.einsum('bhs,bhsv,bhsd->bhvd', weights, values_f, scaled, precision=HI...  9.09 us
    ppermute x2, starting transfers between devices, sizes_trace(): lax.ppermute(f_next, comm_axis, [(rr, rr ^ b) for rr in range(sides)])  4.67 us
    dot_general x1, matrix products, cell_block(): jnp.einsum('bhvd,bhtd->bhtv', state_c, queries, precision=HIGHEST)  3.35 us
    another operation x1, other arithmetic, replay(): jnp.cumsum(masked, axis=-1)  2.76 us
    another operation x1, other arithmetic, cell_block(): cumul = jnp.cumsum(forget, axis=-1)  2.75 us
  transfers between devices with their start and end apart: 2, of which 2 were waited for; matrix products, arithmetic and copies ran while one was open for 1% of the time, Pallas kernels for 0%

profile of v1, /device:TPU:0, one launch (start us, length us, event | category | flops | bytes accessed | tf_op | source)
XLA Modules:
  0.0 130.2 jit_solution(9464848634471605944)
XLA Ops:
  0.7 0.8 add.114
  1.5 0.7 iota_compare_fusion
  2.2 0.7 bitcast_convert_fusion
  2.9 0.8 copy.77
  3.6 1.4 %fusion.7 = f32[16,4]{1,0:T(8,128)S(1)} fusion(bf16[16,4,4096]{2,1,0:T(4,128)(2,1)} %param.17), kind=kLoop, calls=%fused_computation.16 | loop fusion | flops 786368 | bytes 524544 | tf_op jit(solution)/shard_map/reduce_sum | solution.py:118
  5.0 0.7 convert_element_type.41
  5.7 0.7 fusion.41
  6.5 0.1 copy.93
  6.6 0.1 copy.76
  6.7 1.4 %fusion.9 = bf16[16,4,4096]{2,1,0:T(4,128)(2,1)S(1)} fusion(bf16[16,4,4096]{2,1,0:T(4,128)(2,1)} %param.17, f32[4096]{0:T(1024)S(1)} %convert_element_type.41, f32[16,4]{1,0:T(8,128)S(1)} %add_rsqrt_fusion), kind=kLoop, calls=%fused_computation.18 | loop fusion | flops 1048576 | bytes 1065216 | tf_op jit(solution)/shard_map/convert_element_type | solution.py:119
  8.1 0.1 reshape.103
  8.2 0.3 convolution_add_fusion
  8.5 0.1 reshape.104
  8.6 0.1 reshape.105
  8.7 0.1 fusion.24
  8.8 0.1 fusion.39
  8.9 2.8 %reduce_window_sum.18 = f32[16,4,4]{2,1,0:T(4,128)S(1)} reduce-window(f32[16,4,4]{2,1,0:T(4,128)S(1)} %get-tuple-element.26, f32[]{:T(128)} %constant.13.clone.1), window={size=1x1x4 pad=0_0x0_0x3_0}, to_apply=%region_3.4 | reduce-window | flops 768 | bytes 2052 | tf_op jit(solution)/shard_map/jit(cumsum)/reduce_window_sum | solution.py:49
  11.7 2.7 %reduce_window_sum.17 = f32[16,4,4]{2,1,0:T(4,128)S(1)} reduce-window(f32[16,4,4]{2,1,0:T(4,128)S(1)} %fusion.24, f32[]{:T(128)} %constant.13.clone.1), window={size=1x1x4 pad=0_0x0_0x3_0}, to_apply=%region_1.2 | reduce-window | flops 768 | bytes 2052 | tf_op jit(solution)/shard_map/jit(cumsum)/reduce_window_sum | solution.py:65
  14.4 3.0 %convolution_convert_fusion.1 = bf16[64,512]{1,0:T(8,128)(2,1)S(1)} fusion(bf16[64,4096]{1,0:T(8,128)(2,1)S(1)} %reshape.103, bf16[4096,512]{1,0:T(8,128)(2,1)} %param.21), kind=kOutput, calls=%fused_computation.12 | convolution fusion | flops 268468224 | bytes 4784128 | tf_op jit(solution)/shard_map/dot_general | solution.py:123
  17.5 3.1 %convolution_convert_fusion.2 = bf16[64,512]{1,0:T(8,128)(2,1)S(1)} fusion(bf16[64,4096]{1,0:T(8,128)(2,1)S(1)} %reshape.103, bf16[4096,512]{1,0:T(8,128)(2,1)} %param.20), kind=kOutput, calls=%fused_computation.13 | convolution fusion | flops 268468224 | bytes 4784128 | tf_op jit(solution)/shard_map/dot_general | solution.py:123
  20.6 3.1 %convolution_convert_fusion.3 = bf16[64,512]{1,0:T(8,128)(2,1)S(1)} fusion(bf16[64,4096]{1,0:T(8,128)(2,1)S(1)} %reshape.103, bf16[4096,512]{1,0:T(8,128)(2,1)} %param.19), kind=kOutput, calls=%fused_computation.14 | convolution fusion | flops 268468224 | bytes 4784128 | tf_op jit(solution)/shard_map/dot_general | solution.py:123
  23.7 0.2 fusion.38
  23.9 0.2 fusion.16
  24.1 0.1 subtract_exponential_fusion.1
  24.2 0.6 fusion.13
  24.9 0.1 multiply_add_fusion.1
  25.0 0.3 fusion.22
  25.3 0.5 fusion.42
  25.8 0.1 exponential_maximum_fusion
  25.9 0.1 fusion.29
  26.0 9.1 %multiply_add_fusion = f32[16,4,128,128]{3,2,1,0:T(8,128)S(1)} fusion(f32[16,4,128,128]{3,2,1,0:T(8,128)} %param.27, f32[16,4]{1,0:T(8,128)S(1)} %get-tuple-element.23, bf16[16,4,4,128]{3,2,1,0:T(4,128)(2,1)S(1)} %copy-done.4, bf16[16,4,4,128]{3,2,1,0:T(4,128)(2,1)S(1)} %copy-done.5, f32[16,4,4]{2,1,0:T(4,128)S(1)} %get-tuple-element.33), kind=kOutput, calls=%fused_computation | convolution fusion | flops 52559872 | bytes 8520960 | tf_op jit(solution)/shard_map/bhs,bhsv,bhsd->bhvd/dot_general | solution.py:54
  35.2 3.3 %fusion.23 = f32[16,4,4,128]{3,2,1,0:T(4,128)S(1)} fusion(f32[16,4,128,128]{3,2,1,0:T(8,128)S(1)} %multiply_add_fusion, bf16[16,4,4,128]{3,2,1,0:T(4,128)(2,1)S(1)} %reshape.106), kind=kOutput, calls=%fused_computation.44 | convolution fusion | flops 50331648 | bytes 4390912 | tf_op jit(solution)/shard_map/bhvd,bhtd->bhtv/dot_general | solution.py:76
  38.5 0.6 fusion.17
  39.2 0.3 multiply_multiply_fusion
  39.5 0.9 fusion.6
  40.4 0.2 broadcast_in_dim.52
  40.6 36.7 %all_to_all.5 = bf16[32,64,512]{2,1,0:T(8,128)(2,1)S(1)} all-to-all(bf16[32,64,512]{2,1,0:T(8,128)(2,1)S(1)} %broadcast_in_dim.52), channel_id=1, replica_groups=mesh['kv'=32,'tp'=4] {'kv'}, dimensions={0} | all-to-all | bytes 4194304 | tf_op jit(solution)/shard_map/all_to_all | solution.py:31
  77.3 0.7 fusion.43
  78.0 1.6 %collective-permute-start = (f32[2048,128]{1,0:T(8,128)S(1)}, f32[2048,128]{1,0:T(8,128)S(1)}, u32[]{:S(2)}, u32[]{:S(2)}) collective-permute-start(f32[2048,128]{1,0:T(8,128)S(1)} %fusion.43), channel_id=1, source_target_pairs={{0,1},{1,0},{2,3},{3,2},{4,5},{5,4},{6,7},{7,6},{8,9},{9,8},{10,11... | collective-permute-start | bytes 3145736 | tf_op jit(solution)/shard_map/ppermute | solution.py:15
  79.6 23.7 %collective-permute-done = f32[2048,128]{1,0:T(8,128)S(1)} collective-permute-done((f32[2048,128]{1,0:T(8,128)S(1)}, f32[2048,128]{1,0:T(8,128)S(1)}, u32[]{:S(2)}, u32[]{:S(2)}) %collective-permute-start) | collective-permute-done | bytes 1048608 | tf_op jit(solution)/shard_map/ppermute | solution.py:15
  103.3 0.1 add.137
  103.4 3.1 %collective-permute-start.1 = (f32[2048,128]{1,0:T(8,128)S(1)}, f32[2048,128]{1,0:T(8,128)S(1)}, u32[]{:S(2)}, u32[]{:S(2)}) collective-permute-start(f32[2048,128]{1,0:T(8,128)S(1)} %add.137), channel_id=1, source_target_pairs={{0,2},{1,3},{2,0},{3,1},{4,6},{5,7},{6,4},{7,5},{8,10},{9,11},{10,... | collective-permute-start | bytes 3145736 | tf_op jit(solution)/shard_map/ppermute | solution.py:15
  106.5 0.7 copy.87
  107.2 0.1 copy.85
  107.3 0.1 copy.86
  107.4 0.6 pad_maximum_fusion
  108.0 21.3 %collective-permute-done.1 = f32[2048,128]{1,0:T(8,128)S(1)} collective-permute-done((f32[2048,128]{1,0:T(8,128)S(1)}, f32[2048,128]{1,0:T(8,128)S(1)}, u32[]{:S(2)}, u32[]{:S(2)}) %collective-permute-start.1) | collective-permute-done | bytes 1048608 | tf_op jit(solution)/shard_map/ppermute | solution.py:15
  129.3 0.9 add_convert_fusion
  (32 shorter events, 0.3 us)
Async XLA Ops:
  0.6 7.6 %copy-start = (bf16[4096,32]{0,1:T(8,128)(2,1)S(1)}, bf16[4096,32]{0,1:T(8,128)(2,1)}, u32[]{:S(2)}) copy-start(bf16[4096,32]{0,1:T(8,128)(2,1)} %param.23) | copy-start | bytes 786436
  17.5 6.7 %copy-start.4 = (bf16[16,4,4,128]{3,2,1,0:T(4,128)(2,1)S(1)}, bf16[16,4,4,128]{3,2,1,0:T(4,128)(2,1)}, u32[]{:S(2)}) copy-start(bf16[16,4,4,128]{3,2,1,0:T(4,128)(2,1)} %param.30) | copy-start | bytes 196612
  20.6 4.3 %copy-start.8 = (f32[16,4,128]{2,1,0:T(4,128)S(1)}, f32[16,4,128]{2,1,0:T(4,128)}, u32[]{:S(2)}) copy-start(f32[16,4,128]{2,1,0:T(4,128)} %param.28) | copy-start | bytes 98308
  20.6 5.4 %copy-start.5 = (bf16[16,4,4,128]{3,2,1,0:T(4,128)(2,1)S(1)}, bf16[16,4,4,128]{3,2,1,0:T(4,128)(2,1)}, u32[]{:S(2)}) copy-start(bf16[16,4,4,128]{3,2,1,0:T(4,128)(2,1)} %param.31) | copy-start | bytes 196612
  24.9 10.3 %copy-start.7 = (bf16[16,4,4,128]{3,2,1,0:T(4,128)(2,1)}, bf16[16,4,4,128]{3,2,1,0:T(4,128)(2,1)S(1)}, u32[]{:S(2)}) copy-start(bf16[16,4,4,128]{3,2,1,0:T(4,128)(2,1)S(1)} %get-tuple-element.40) | copy-start | bytes 196612
  24.9 13.7 %copy-start.6 = (bf16[16,4,4,128]{3,2,1,0:T(4,128)(2,1)}, bf16[16,4,4,128]{3,2,1,0:T(4,128)(2,1)S(1)}, u32[]{:S(2)}) copy-start(bf16[16,4,4,128]{3,2,1,0:T(4,128)(2,1)S(1)} %get-tuple-element.39) | copy-start | bytes 196612
  25.0 10.2 %copy-start.9 = (f32[16,4,128]{2,1,0:T(4,128)}, f32[16,4,128]{2,1,0:T(4,128)S(1)}, u32[]{:S(2)}) copy-start(f32[16,4,128]{2,1,0:T(4,128)S(1)} %multiply_add_fusion.1) | copy-start | bytes 98308
  35.1 5.2 %copy-start.1 = (f32[16,4,128,128]{3,2,1,0:T(8,128)}, f32[16,4,128,128]{3,2,1,0:T(8,128)S(1)}, u32[]{:S(2)}) copy-start(f32[16,4,128,128]{3,2,1,0:T(8,128)S(1)} %multiply_add_fusion) | copy-start | bytes 12582916
  35.2 4.3 %copy-start.2 = (bf16[4096,512]{1,0:T(8,128)(2,1)S(1)}, bf16[4096,512]{1,0:T(8,128)(2,1)}, u32[]{:S(2)}) copy-start(bf16[4096,512]{1,0:T(8,128)(2,1)} %param.22) | copy-start | bytes 12582916
  40.4 36.9 %copy-start.3 = (bf16[512,128]{1,0:T(8,128)(2,1)S(1)}, bf16[512,128]{1,0:T(8,128)(2,1)}, u32[]{:S(2)}) copy-start(bf16[512,128]{1,0:T(8,128)(2,1)} %param.26) | copy-start | bytes 393220
  78.0 25.3 %collective-permute-start = (f32[2048,128]{1,0:T(8,128)S(1)}, f32[2048,128]{1,0:T(8,128)S(1)}, u32[]{:S(2)}, u32[]{:S(2)}) collective-permute-start(f32[2048,128]{1,0:T(8,128)S(1)} %fusion.43), channel_id=1, source_target_pairs={{0,1},{1,0},{2,3},{3,2},{4,5},{5,4},{6,7},{7,6},{8,9},{9,8},{10,11... | collective-permute-start | bytes 3145736 | tf_op jit(solution)/shard_map/ppermute | solution.py:15
  103.4 25.9 %collective-permute-start.1 = (f32[2048,128]{1,0:T(8,128)S(1)}, f32[2048,128]{1,0:T(8,128)S(1)}, u32[]{:S(2)}, u32[]{:S(2)}) collective-permute-start(f32[2048,128]{1,0:T(8,128)S(1)} %add.137), channel_id=1, source_target_pairs={{0,2},{1,3},{2,0},{3,1},{4,6},{5,7},{6,4},{7,5},{8,10},{9,11},{10,... | collective-permute-start | bytes 3145736 | tf_op jit(solution)/shard_map/ppermute | solution.py:15
